TPU v7x, 32 devices: a whole 2x2x4 slice. The times are simulated.
32 devices in a mesh: ep: 8 (over z, core), tp: 4 (over y, x).
Axes of the slice: x: 2, y: 2, z: 4, core: 2. Of those that a mesh axis runs over, the one named last changes fastest.
Arguments:
- stream: bfloat16 [128, 4096], P('ep'), may hold values from -6 to 6
- previous_state: float32 [128, 128, 4096], P('ep', None, 'tp'), may hold values from -6 to 6
- mixer_norm_gain: float32 [4096], replicated, may hold values from 0.1 to 1.9
- query_matrix: bfloat16 [4096, 2048], P('ep'), may hold values from -0.09375 to 0.09375
- key_matrix: bfloat16 [4096, 2048], P('ep'), may hold values from -0.09375 to 0.09375
- value_matrix: bfloat16 [4096, 4096], P('ep', 'tp'), may hold values from -0.09375 to 0.09375
- output_gate_weight: bfloat16 [4096, 4096], P('ep', 'tp'), may hold values from -0.09375 to 0.09375
- decay_lower_factor: bfloat16 [4096, 64], replicated, may hold values from -0.09375 to 0.09375
- decay_upper_factor: bfloat16 [64, 2048], replicated, may hold values from -3 to 3
- forgetting_boost: float32 [128, 2048], P('ep'), may hold values from 0.02 to 1.5
- head_norm_gain: float32 [256], replicated, may hold values from 0.1 to 1.9
- output_matrix: bfloat16 [4096, 4096], P('tp'), may hold values from -0.1875 to 0.1875
- mixture_norm_gain: float32 [4096], replicated, may hold values from 0.1 to 1.9
- expert_gate_weight: bfloat16 [8, 1024, 4096], P('ep', 'tp'), may hold values from -0.09375 to 0.09375
- expert_up_weight: bfloat16 [8, 1024, 4096], P('ep', 'tp'), may hold values from -0.09375 to 0.09375
- expert_down_weight: bfloat16 [8, 1024, 4096], P('ep', None, 'tp'), may hold values from -0.375 to 0.375
- expert_index_table: int32 [128, 2], P('ep'), may hold values from 0 to 7, as said below
- expert_scores_within: float32 [128, 2], P('ep'), may hold values from -6 to 6
- group_probability: float32 [128], P('ep'), may hold values from 0.3 to 1
Outputs:
- new_stream: bfloat16 [128, 4096], P('ep', 'tp')
- new_state: float32 [128, 128, 4096], P('ep', None, 'tp')
Inputs may be any that keep to these rules, and one draw needn't show every extreme that they name: `expert_index_table`: the 2 experts of a sequence are distinct and lie in one group of 2 consecutive experts. Among the 16 sequences of one index of ep (aligned blocks of rows), each expert is named at most 8 times, and in every block some experts are named exactly 8 times.
All inputs are finite; a program needn't handle non-finite values.
Results may differ from a plain program's by a relative error of at most 0.02.
Values may be sent and summed in bfloat16 or wider, within the bound.
A program may use at most 128 MiB of HBM per device.

v0:
```python
import jax
import jax.numpy as jnp
from jax import lax
from jax.sharding import PartitionSpec as P

HEAD_TOTAL = 16
KEY_CHANNELS = 128
DV = 256
epsilon = 1e-06
forgetting_softness = 16.0


def rms_scaled(values, gain_vec):
    floats = values.astype(jnp.float32)
    scaled = floats * lax.rsqrt(jnp.mean(floats * floats, axis=-1, keepdims=True) + epsilon)
    return (scaled * gain_vec).astype(jnp.bfloat16)


def on_device(
    stream,
    previous_state,
    mixer_norm_gain,
    query_matrix,
    key_matrix,
    value_matrix,
    output_gate_weight,
    decay_lower_factor,
    decay_upper_factor,
    forgetting_boost,
    head_norm_gain,
    output_matrix,
    mixture_norm_gain,
    expert_gate_weight,
    expert_up_weight,
    expert_down_weight,
    expert_index_table,
    expert_scores_within,
    group_probability,
):
    seq_count, model_width = stream.shape
    value_local = previous_state.shape[2]
    head_count = max(1, value_local // DV)
    head_width = min(value_local, DV)
    tp_index = lax.axis_index("tp")
    leading_head = tp_index * value_local // DV
    value_start = tp_index * value_local % DV
    key_column_span = head_count * KEY_CHANNELS
    normed = rms_scaled(stream, mixer_norm_gain)
    own_query = lax.dynamic_slice_in_dim(
        query_matrix, leading_head * KEY_CHANNELS, key_column_span, 1
    )
    own_key = lax.dynamic_slice_in_dim(key_matrix, leading_head * KEY_CHANNELS, key_column_span, 1)
    spread = lax.all_to_all(normed, "ep", split_axis=1, concat_axis=0, tiled=True)
    joined = jnp.concatenate([own_query, own_key, value_matrix, output_gate_weight], axis=1)
    summed = lax.psum_scatter(
        jnp.dot(spread, joined, preferred_element_type=jnp.float32),
        "ep",
        scatter_dimension=0,
        tiled=True,
    )
    query_sum = summed[:, :key_column_span]
    key_sum = summed[:, key_column_span : 2 * key_column_span]
    value_sum = summed[:, 2 * key_column_span : 2 * key_column_span + value_local]
    gate_sum = summed[:, 2 * key_column_span + value_local :]
    queries = (query_sum * KEY_CHANNELS ** (-0.5)).astype(jnp.bfloat16)
    key_rows = key_sum.astype(jnp.bfloat16)
    value_rows = value_sum.astype(jnp.bfloat16)
    gate_rows = gate_sum.astype(jnp.bfloat16)
    low_rank = jnp.dot(normed, decay_lower_factor, preferred_element_type=jnp.float32).astype(
        jnp.bfloat16
    )
    local_expand_matrix = lax.dynamic_slice_in_dim(
        decay_upper_factor, leading_head * KEY_CHANNELS, key_column_span, 1
    )
    forgetting_logit = jnp.dot(low_rank, local_expand_matrix, preferred_element_type=jnp.float32)
    request_boost = lax.dynamic_slice_in_dim(
        forgetting_boost, leading_head * KEY_CHANNELS, key_column_span, 1
    )
    forgetting_lograte = jax.nn.log_sigmoid(forgetting_logit) / forgetting_softness - request_boost
    factor = (
        jnp.exp(forgetting_lograte)
        .reshape(seq_count, head_count, KEY_CHANNELS)
        .transpose(0, 2, 1)[..., None]
    )
    state_four = previous_state.reshape(seq_count, KEY_CHANNELS, head_count, head_width)
    key_part = (
        key_rows.astype(jnp.float32)
        .reshape(seq_count, head_count, KEY_CHANNELS)
        .transpose(0, 2, 1)[..., None]
    )
    value_part = value_rows.astype(jnp.float32).reshape(seq_count, 1, head_count, head_width)
    updated = factor * state_four + key_part * value_part
    query_part = (
        queries.astype(jnp.float32).reshape(seq_count, head_count, KEY_CHANNELS).transpose(0, 2, 1)
    )
    readout = jnp.einsum("skh,skhv->shv", query_part, updated, precision=lax.Precision.HIGHEST)
    square_sums = jnp.sum(readout * readout, axis=-1)
    norm_table = lax.dynamic_update_slice(
        jnp.zeros((seq_count, HEAD_TOTAL), jnp.float32), square_sums, (jnp.int32(0), leading_head)
    )
    totals = lax.psum(norm_table, "tp")
    own_totals = lax.dynamic_slice_in_dim(totals, leading_head, head_count, 1)
    mean_sq = own_totals[..., None] / DV
    own_gain = lax.dynamic_slice_in_dim(head_norm_gain, value_start, head_width, 0)
    gate_part = jax.nn.silu(
        gate_rows.astype(jnp.float32).reshape(seq_count, head_count, head_width)
    )
    gated_rows = (
        (readout * lax.rsqrt(mean_sq + epsilon) * own_gain * gate_part)
        .reshape(seq_count, value_local)
        .astype(jnp.bfloat16)
    )
    partial_out = jnp.dot(gated_rows, output_matrix, preferred_element_type=jnp.float32)
    mixer_sum = lax.psum(partial_out.astype(jnp.bfloat16), "tp").astype(jnp.float32)
    blended_tokens = (stream.astype(jnp.float32) + mixer_sum).astype(jnp.bfloat16)
    normed_two = rms_scaled(blended_tokens, mixture_norm_gain)
    ep_count = lax.axis_size("ep")
    local_experts = expert_gate_weight.shape[0]
    experts_all = ep_count * local_experts
    route_count = expert_index_table.shape[1]
    capacity = 2 * seq_count * route_count // experts_all
    slot_count = experts_all * capacity
    flat_ids = expert_index_table.reshape(seq_count * route_count)
    one_hot = (flat_ids[:, None] == jnp.arange(experts_all, dtype=jnp.int32)[None, :]).astype(
        jnp.int32
    )
    rank_in = jnp.sum(one_hot * (jnp.cumsum(one_hot, axis=0) - 1), axis=1)
    place_lookup = flat_ids * capacity + rank_in
    placing = (place_lookup[:, None] == jnp.arange(slot_count, dtype=jnp.int32)[None, :]).astype(
        jnp.float32
    )
    placing = placing.reshape(seq_count, route_count, slot_count)
    logit_exp = jnp.exp(expert_scores_within)
    weights = logit_exp / jnp.sum(logit_exp, axis=-1, keepdims=True) * group_probability[:, None]
    combine = jnp.einsum("sk,skc->sc", weights, placing, precision=lax.Precision.HIGHEST)
    dispatch = jnp.sum(placing, axis=1).astype(jnp.bfloat16)
    outgoing = jnp.einsum("sc,sd->cd", dispatch, normed_two, preferred_element_type=jnp.float32)
    outgoing = outgoing.astype(jnp.bfloat16).reshape(experts_all, capacity, model_width)
    width_local = expert_down_weight.shape[2]
    arrived = lax.all_to_all(outgoing, "ep", split_axis=0, concat_axis=0, tiled=True)
    held_slots = arrived.shape[1]
    grouped = arrived.reshape(ep_count, local_experts, held_slots, model_width)
    gate_pre = jnp.einsum(
        "sxcd,xfd->sxcf", grouped, expert_gate_weight, preferred_element_type=jnp.float32
    )
    up_pre = jnp.einsum(
        "sxcd,xfd->sxcf", grouped, expert_up_weight, preferred_element_type=jnp.float32
    )
    hidden = (jax.nn.silu(gate_pre) * up_pre).astype(jnp.bfloat16)
    outputs = jnp.einsum(
        "sxcf,xfd->sxcd",
        lax.all_gather(hidden, "tp", axis=3, tiled=True),
        expert_down_weight,
        preferred_element_type=jnp.float32,
    )
    ready_rows = outputs.astype(jnp.bfloat16).reshape(
        ep_count * local_experts, held_slots, width_local
    )
    returned = lax.all_to_all(ready_rows, "ep", split_axis=0, concat_axis=0, tiled=True)
    mixture = jnp.dot(
        combine,
        returned.reshape(slot_count, width_local).astype(jnp.float32),
        precision=lax.Precision.HIGHEST,
    )
    own_mixed = lax.dynamic_slice_in_dim(blended_tokens, tp_index * width_local, width_local, 1)
    new_stream = (own_mixed.astype(jnp.float32) + mixture).astype(jnp.bfloat16)
    return (new_stream, updated.reshape(seq_count, KEY_CHANNELS, value_local))


def solution(mesh):
    placed = (
        P("ep", None),
        P("ep", None, "tp"),
        P(),
        P("ep", None),
        P("ep", None),
        P("ep", "tp"),
        P("ep", "tp"),
        P(),
        P(),
        P("ep", None),
        P(),
        P("tp", None),
        P(),
        P("ep", "tp", None),
        P("ep", "tp", None),
        P("ep", None, "tp"),
        P("ep", None),
        P("ep", None),
        P("ep"),
    )
    return jax.shard_map(
        on_device,
        mesh=mesh,
        in_specs=placed,
        out_specs=(P("ep", "tp"), P("ep", None, "tp")),
        check_vma=False,
    )
```

profile of v0, /device:TPU:1, one launch (start us, length us, event | category | flops | bytes accessed | tf_op | source)
XLA Modules:
  0.0 207.3 jit_solution(5548687518825373681)
XLA Ops:
  7.2 1.2 fusion.36
  8.4 1.0 fusion.38
  9.4 0.7 copy.61
  10.1 6.4 %all-to-all-start = ((bf16[16,8,512]{2,0,1:T(8,128)(2,1)}), bf16[16,8,512]{2,0,1:T(8,128)(2,1)S(1)}, u32[]{:S(2)}, u32[]{:S(2)}) async-start(bf16[16,8,512]{2,0,1:T(8,128)(2,1)} %bitcast.84), calls=%async_computation | async-start | bytes 262144 | tf_op jit(solution)/shard_map/all_to_all | solution.py:53
  16.4 1.3 constant_dynamic-slice_fusion
  17.7 4.5 %all-to-all-done = bf16[16,8,512]{2,0,1:T(8,128)(2,1)S(1)} async-done(((bf16[16,8,512]{2,0,1:T(8,128)(2,1)}), bf16[16,8,512]{2,0,1:T(8,128)(2,1)S(1)}, u32[]{:S(2)}, u32[]{:S(2)}) %all-to-all-start) | async-done | bytes 131104 | tf_op jit(solution)/shard_map/all_to_all | solution.py:53
  22.2 3.3 %fusion.3 = f32[128,3072]{1,0:T(8,128)} fusion(bf16[128,512]{1,0:T(8,128)(2,1)S(1)} %bitcast.90, bf16[512,1024]{1,0:T(8,128)(2,1)} %param.25, bf16[512,1024]{1,0:T(8,128)(2,1)} %param.24, bf16[512,512]{1,0:T(8,128)(2,1)S(1)} %get-tuple-element.6, bf16[512,512]{1,0:T(8,128)(2,1)S(1)} %get-tuple-element.7), kind=kOutput, calls=%fused_computation.7 | convolution fusion | flops 415236096 | bytes 4849664 | tf_op jit(solution)/shard_map/dot_general | solution.py:56
  26.3 10.6 %reshape.119 = f32[16,128,4,256]{3,2,1,0:T(4,128)} reshape(f32[16,128,1024]{2,1,0:T(8,128)} %param.20) | data formatting | bytes 16777216 | tf_op jit(solution)/shard_map/reshape | solution.py:85
  36.9 1.3 fusion.53
  38.6 17.5 %reduce-scatter.2.cloned.1.call-done = f32[16,3072]{1,0:T(8,128)} async-done(((f32[128,3072]{1,0:T(8,128)}), f32[16,3072]{1,0:T(8,128)}) %reduce-scatter.2.cloned.1.call-update) | async-done | bytes 196624 | tf_op jit(solution)/shard_map/reduce_scatter | solution.py:55
  56.1 0.9 convert.8
  57.1 1.4 copy.41
  58.6 0.8 fusion.54
  59.4 6.4 %multiply_add_fusion.1 = f32[16,128,4,256]{3,2,1,0:T(4,128)S(1)} fusion(f32[16,128,4,256]{3,2,1,0:T(4,128)} %reshape.119, f32[16,4,256]{2,1,0:T(4,128)S(1)} %mul.156, f32[16,128,4]{2,1,0:T(8,128)} %copy.41, f32[16,128,4]{2,1,0:T(8,128)S(1)} %copy.40), kind=kLoop, calls=%fused_computation.3 | loop fusion | flops 6291456 | bytes 16908288 | tf_op jit(solution)/shard_map/add | solution.py:92
  65.8 3.4 %fusion = f32[16,4,1,256]{3,2,1,0:T(1,128)S(1)} fusion(f32[16,128,4,256]{3,2,1,0:T(4,128)S(1)} %multiply_add_fusion.1, bf16[16,128,4,1]{1,2,0,3:T(4,128)(2,1)S(1)} %bitcast.87), kind=kOutput, calls=%fused_computation | convolution fusion | flops 25165824 | bytes 8470528 | tf_op jit(solution)/shard_map/skh,skhv->shv/dot_general | solution.py:96
  69.5 8.3 %psum.14 = f32[16,16]{1,0:T(8,128)S(1)} all-reduce(f32[16,16]{1,0:T(8,128)S(1)} %dynamic_update_slice.3), channel_id=1, replica_groups=mesh['ep'=8,'tp'=4] {'tp'}, use_global_device_ids=true, to_apply=%region_3.4 | all-reduce | flops 256 | bytes 2048 | tf_op jit(solution)/shard_map/psum | solution.py:101
  78.0 5.3 %convolution_convert_fusion.1 = bf16[16,4096]{1,0:T(8,128)(2,1)} fusion(bf16[16,1024]{1,0:T(8,128)(2,1)S(1)} %bitcast.86, bf16[1024,4096]{1,0:T(8,128)(2,1)} %param.30), kind=kOutput, calls=%fused_computation.6 | convolution fusion | flops 134283264 | bytes 8552448 | tf_op jit(solution)/shard_map/dot_general | solution.py:113
  83.5 43.3 %all-reduce.2.cloned.1.call-done = bf16[16,4096]{1,0:T(8,128)(2,1)} async-done(((bf16[16,4096]{1,0:T(8,128)(2,1)}), bf16[16,4096]{1,0:T(8,128)(2,1)}) %all-reduce.2.cloned.1.call-update) | async-done | bytes 131088 | tf_op jit(solution)/shard_map/psum | solution.py:114
  126.8 1.1 fusion.33
  127.9 1.2 fusion.2
  129.0 5.7 %all-to-all-start.1 = ((bf16[8,8,4096]{2,1,0:T(8,128)(2,1)}), bf16[8,8,4096]{2,1,0:T(8,128)(2,1)}, u32[]{:S(2)}, u32[]{:S(2)}) async-start(bf16[8,8,4096]{2,1,0:T(8,128)(2,1)} %fusion.2), calls=%async_computation.2 | async-start | bytes 1048576 | tf_op jit(solution)/shard_map/all_to_all | solution.py:140
  134.8 4.5 %mul.153 = f32[16,128,4,256]{3,2,1,0:T(4,128)} broadcast(f32[16,128,4]{2,1,0:T(8,128)S(1)} %copy.40), dimensions={0,1,2} | broadcast | bytes 8421376 | tf_op jit(solution)/shard_map/mul | solution.py:92
  139.4 10.8 %mul.178 = f32[16,128,1024]{2,1,0:T(8,128)} reshape(f32[16,128,4,256]{3,2,1,0:T(4,128)} %mul.153) | data formatting | bytes 16777216 | tf_op jit(solution)/shard_map/mul | solution.py:92
  150.5 4.6 %mul.155 = f32[16,128,4,256]{3,2,1,0:T(4,128)} broadcast(f32[16,128,4]{2,1,0:T(8,128)S(1)} %copy-done.1), dimensions={0,1,2} | broadcast | bytes 8421376 | tf_op jit(solution)/shard_map/mul | solution.py:92
  155.1 10.7 %mul.180 = f32[16,128,1024]{2,1,0:T(8,128)} reshape(f32[16,128,4,256]{3,2,1,0:T(4,128)} %mul.155) | data formatting | bytes 16777216 | tf_op jit(solution)/shard_map/mul | solution.py:92
  165.8 2.5 %fusion.20 = f32[8,1,8,256]{3,2,0,1:T(8,128)S(1)} fusion(bf16[8,8,4096]{2,1,0:T(8,128)(2,1)} %all-to-all-done.1, bf16[1,256,4096]{2,1,0:T(8,128)(2,1)} %param.32), kind=kOutput, calls=%fused_computation.23 | convolution fusion | flops 134217728 | bytes 2686976 | tf_op jit(solution)/shard_map/sxcd,xfd->sxcf/dot_general | solution.py:143
  168.3 2.5 %fusion.29 = bf16[8,1,8,256]{3,2,0,1:T(8,128)(2,1)S(1)} fusion(bf16[8,8,4096]{2,1,0:T(8,128)(2,1)} %all-to-all-done.1, bf16[1,256,4096]{2,1,0:T(8,128)(2,1)} %param.33, f32[8,1,8,256]{3,2,0,1:T(8,128)S(1)} %fusion.20), kind=kOutput, calls=%fused_computation.26 | convolution fusion | flops 134316032 | bytes 2719744 | tf_op jit(solution)/shard_map/sxcd,xfd->sxcf/dot_general | solution.py:146
  170.9 6.9 %all_gather.3 = bf16[8,1,8,1024]{3,2,0,1:T(8,128)(2,1)S(1)} all-gather(bf16[8,1,8,256]{3,2,0,1:T(8,128)(2,1)S(1)} %fusion.29), channel_id=1, replica_groups=mesh['ep'=8,'tp'=4] {'tp'}, dimensions={3}, use_global_device_ids=true | all-gather | bytes 163840 | tf_op jit(solution)/shard_map/all_gather | solution.py:152
  177.8 1.1 fusion.17
  178.9 7.1 %all-to-all-start.2 = ((bf16[8,8,1024]{2,1,0:T(8,128)(2,1)}), bf16[8,8,1024]{2,1,0:T(8,128)(2,1)S(1)}, u32[]{:S(2)}, u32[]{:S(2)}) async-start(bf16[8,8,1024]{2,1,0:T(8,128)(2,1)} %fusion.17), calls=%async_computation.3 | async-start | bytes 262144 | tf_op jit(solution)/shard_map/all_to_all | solution.py:159
  186.0 13.6 %multiply_add_fusion = f32[16,128,1024]{2,1,0:T(8,128)} fusion(f32[16,128,1024]{2,1,0:T(8,128)} %mul.180, f32[16,128,1024]{2,1,0:T(8,128)} %mul.178, f32[16,128,1024]{2,1,0:T(8,128)} %param.20, f32[16,1024]{1,0:T(8,128)S(1)} %get-tuple-element.4), kind=kLoop, calls=%fused_computation.2 | loop fusion | flops 6291456 | bytes 33619968 | tf_op jit(solution)/shard_map/add | solution.py:92
  199.6 0.8 fusion.32
  (54 shorter events, 2.3 us)
Async XLA Ops:
  7.2 170.6 %copy-start = (bf16[1,1024,1024]{2,1,0:T(8,128)(2,1)S(1)}, bf16[1,1024,1024]{2,1,0:T(8,128)(2,1)}, u32[]{:S(2)}) copy-start(bf16[1,1024,1024]{2,1,0:T(8,128)(2,1)} %param.34) | copy-start | bytes 6291460
  10.1 12.1 %all-to-all-start = ((bf16[16,8,512]{2,0,1:T(8,128)(2,1)}), bf16[16,8,512]{2,0,1:T(8,128)(2,1)S(1)}, u32[]{:S(2)}, u32[]{:S(2)}) async-start(bf16[16,8,512]{2,0,1:T(8,128)(2,1)} %bitcast.84), calls=%async_computation | async-start | bytes 262144 | tf_op jit(solution)/shard_map/all_to_all | solution.py:53
  16.4 39.6 %reduce-scatter.2.cloned.1.call-start = ((), (), s32[]{:S(2)}) async-start(), calls=%async_computation.4 | async-start | bytes 1769472 | tf_op jit(solution)/shard_map/reduce_scatter | solution.py:55
  22.2 3.4 %copy-start.5 = (s32[16,2]{0,1:T(2,128)S(1)}, s32[16,2]{0,1:T(2,128)}, u32[]{:S(2)}) copy-start(s32[16,2]{0,1:T(2,128)} %param.35) | copy-start | bytes 388
  25.5 101.2 %all-reduce.2.cloned.1.call-start = ((), (), s32[]{:S(2)}) async-start(), calls=%async_computation.5 | async-start | bytes 262144 | tf_op jit(solution)/shard_map/psum | solution.py:114
  26.3 10.6 %copy-start.3 = (bf16[4096,64]{0,1:T(8,128)(2,1)S(1)}, bf16[4096,64]{0,1:T(8,128)(2,1)}, u32[]{:S(2)}) copy-start(bf16[4096,64]{0,1:T(8,128)(2,1)} %param.26) | copy-start | bytes 1572868
  65.8 12.1 %copy-start.6 = (f32[256]{0:T(256)S(1)}, f32[256]{0:T(256)}, u32[]{:S(2)}) copy-start(f32[256]{0:T(256)} %param.29) | copy-start | bytes 3076
  78.0 48.8 %copy-start.2 = (bf16[16,4096]{1,0:T(8,128)(2,1)S(1)}, bf16[16,4096]{1,0:T(8,128)(2,1)}, u32[]{:S(2)}) copy-start(bf16[16,4096]{1,0:T(8,128)(2,1)} %param.19) | copy-start | bytes 393220
  78.0 49.8 %copy-start.4 = (f32[4096]{0:T(1024)S(1)}, f32[4096]{0:T(1024)}, u32[]{:S(2)}) copy-start(f32[4096]{0:T(1024)} %param.31) | copy-start | bytes 49156
  78.0 56.7 %copy-start.7 = (f32[16,2]{0,1:T(2,128)S(1)}, f32[16,2]{0,1:T(2,128)}, u32[]{:S(2)}) copy-start(f32[16,2]{0,1:T(2,128)} %param.36) | copy-start | bytes 388
  78.0 56.7 %copy-start.8 = (f32[16]{0:T(128)S(1)}, f32[16]{0:T(128)}, u32[]{:S(2)}) copy-start(f32[16]{0:T(128)} %param.37) | copy-start | bytes 196
  129.0 36.8 %all-to-all-start.1 = ((bf16[8,8,4096]{2,1,0:T(8,128)(2,1)}), bf16[8,8,4096]{2,1,0:T(8,128)(2,1)}, u32[]{:S(2)}, u32[]{:S(2)}) async-start(bf16[8,8,4096]{2,1,0:T(8,128)(2,1)} %fusion.2), calls=%async_computation.2 | async-start | bytes 1048576 | tf_op jit(solution)/shard_map/all_to_all | solution.py:140
  139.4 11.1 %copy-start.1 = (f32[16,128,4]{2,1,0:T(8,128)S(1)}, f32[16,128,4]{2,1,0:T(8,128)}, u32[]{:S(2)}) copy-start(f32[16,128,4]{2,1,0:T(8,128)} %copy.41) | copy-start | bytes 98308
  178.9 20.7 %all-to-all-start.2 = ((bf16[8,8,1024]{2,1,0:T(8,128)(2,1)}), bf16[8,8,1024]{2,1,0:T(8,128)(2,1)S(1)}, u32[]{:S(2)}, u32[]{:S(2)}) async-start(bf16[8,8,1024]{2,1,0:T(8,128)(2,1)} %fusion.17), calls=%async_computation.3 | async-start | bytes 262144 | tf_op jit(solution)/shard_map/all_to_all | solution.py:159
Sparse Core Ops, SparseCore 0:
  25.7 30.3 reduce-scatter.1
  83.5 43.2 all-reduce.1
where the time goes:
time: 209 us; the launch traced here: 207 us
  waiting for transfers between devices  65.4 us (31%)
  local copies, waits for them, and re-layouts  45.8 us (22%)
  other arithmetic  25.8 us (12%)
  matrix products  21.6 us (10%)
  starting transfers between devices  19.2 us (9%)
  blocking collectives  15.2 us (7%)
  between operations  14.3 us (7%)
    psum x1, waiting for transfers between devices, on_device(): lax.psum(partial_out.astype(jnp.bfloat16), 'tp').astype(jnp.float32)  43.3 us
    mul x5, local copies, waits for them, and re-layouts, on_device(): updated = factor * state_four + key_part * value_part  30.7 us
    add x2, other arithmetic, on_device(): updated = factor * state_four + key_part * value_part  20 us
    reduce_scatter x1, waiting for transfers between devices, on_device(): lax.psum_scatter(jnp.dot(spread, joined, preferred_element_type=jnp.float...  17.5 us
    reshape x1, local copies, waits for them, and re-layouts, on_device(): previous_state.reshape(seq_count, KEY_CHANNELS, head_count, head_width)  10.6 us
    psum x1, blocking collectives, on_device(): totals = lax.psum(norm_table, 'tp')  8.28 us
    all_to_all x1, starting transfers between devices, on_device(): lax.all_to_all(ready_rows, 'ep', split_axis=0, concat_axis=0, tiled=True)  7.12 us
    all_gather x1, blocking collectives, on_device(): lax.all_gather(hidden, 'tp', axis=3, tiled=True)  6.91 us
  transfers between devices with their start and end apart: 5, of which 3 were waited for; matrix products, arithmetic and copies ran while one was open for 28% of the time, Pallas kernels for 0%

commit v1 on v0

--- a/solution.py
+++ b/solution.py
@@ -111,7 +111,9 @@
         .astype(jnp.bfloat16)
     )
     partial_out = jnp.dot(gated_rows, output_matrix, preferred_element_type=jnp.float32)
-    mixer_sum = lax.psum(partial_out.astype(jnp.bfloat16), "tp").astype(jnp.float32)
+    mixer_sum = jnp.sum(lax.all_gather(partial_out.astype(jnp.bfloat16), "tp"), axis=0).astype(
+        jnp.float32
+    )
     blended_tokens = (stream.astype(jnp.float32) + mixer_sum).astype(jnp.bfloat16)
     normed_two = rms_scaled(blended_tokens, mixture_norm_gain)
     ep_count = lax.axis_size("ep")

time: 209 us -> 180 us (0.86)
  waiting for transfers between devices: 65.4 us -> 22 us
  blocking collectives: 15.2 us -> 23.1 us
  starting transfers between devices: 19.2 us -> 25.1 us
    psum x1 -> x0, waiting for transfers between devices: 43.3 us -> none  [on_device(): lax.psum(partial_out.astype(jnp.bfloat16), 'tp').astype(jnp.float32)]
    all_gather x0 -> x1, blocking collectives: none -> 8.03 us  [on_device(): lax.all_gather(partial_out.astype(jnp.bfloat16), 'tp')]
    all_to_all x1, starting transfers between devices: 5.72 us -> 11.6 us  [on_device(): lax.all_to_all(outgoing, 'ep', split_axis=0, concat_axis=0, tiled=True)]
  transfers between devices with their start and end apart: 5 -> 4, of which waited for: 3 -> 2; matrix products, arithmetic and copies ran while one was open for 28% -> 33% of each run, Pallas kernels for 0% -> 0%
where the time goes in v1:
time: 180 us; the launch traced here: 179 us
  local copies, waits for them, and re-layouts  45.8 us (25%)
  other arithmetic  27.6 us (15%)
  starting transfers between devices  25.1 us (14%)
  blocking collectives  23.1 us (13%)
  waiting for transfers between devices  22 us (12%)
  matrix products  20.9 us (12%)
  between operations  14.3 us (8%)
    mul x5, local copies, waits for them, and re-layouts, on_device(): updated = factor * state_four + key_part * value_part  30.7 us
    add x2, other arithmetic, on_device(): updated = factor * state_four + key_part * value_part  20 us
    reduce_scatter x1, waiting for transfers between devices, on_device(): lax.psum_scatter(jnp.dot(spread, joined, preferred_element_type=jnp.float...  17.5 us
    all_to_all x1, starting transfers between devices, on_device(): lax.all_to_all(outgoing, 'ep', split_axis=0, concat_axis=0, tiled=True)  11.6 us
    reshape x1, local copies, waits for them, and re-layouts, on_device(): previous_state.reshape(seq_count, KEY_CHANNELS, head_count, head_width)  10.6 us
    psum x1, blocking collectives, on_device(): totals = lax.psum(norm_table, 'tp')  8.25 us
    all_gather x1, blocking collectives, on_device(): lax.all_gather(partial_out.astype(jnp.bfloat16), 'tp')  8.03 us
    all_to_all x1, starting transfers between devices, on_device(): lax.all_to_all(ready_rows, 'ep', split_axis=0, concat_axis=0, tiled=True)  7.15 us
  transfers between devices with their start and end apart: 4, of which 2 were waited for; matrix products, arithmetic and copies ran while one was open for 33% of the time, Pallas kernels for 0%

profile of v1, /device:TPU:1, one launch (start us, length us, event | category | flops | bytes accessed | tf_op | source)
XLA Modules:
  0.0 178.9 jit_solution(7231097450512045417)
XLA Ops:
  7.2 1.2 fusion.36
  8.4 1.0 fusion.38
  10.1 6.4 %all-to-all-start = ((bf16[16,8,512]{2,0,1:T(8,128)(2,1)}), bf16[16,8,512]{2,0,1:T(8,128)(2,1)S(1)}, u32[]{:S(2)}, u32[]{:S(2)}) async-start(bf16[16,8,512]{2,0,1:T(8,128)(2,1)} %bitcast.85), calls=%async_computation | async-start | bytes 262144 | tf_op jit(solution)/shard_map/all_to_all | solution.py:53
  16.4 1.3 constant_dynamic-slice_fusion
  17.7 4.5 %all-to-all-done = bf16[16,8,512]{2,0,1:T(8,128)(2,1)S(1)} async-done(((bf16[16,8,512]{2,0,1:T(8,128)(2,1)}), bf16[16,8,512]{2,0,1:T(8,128)(2,1)S(1)}, u32[]{:S(2)}, u32[]{:S(2)}) %all-to-all-start) | async-done | bytes 131104 | tf_op jit(solution)/shard_map/all_to_all | solution.py:53
  22.2 3.3 %fusion.3 = f32[128,3072]{1,0:T(8,128)} fusion(bf16[128,512]{1,0:T(8,128)(2,1)S(1)} %bitcast.92, bf16[512,1024]{1,0:T(8,128)(2,1)} %param.25, bf16[512,1024]{1,0:T(8,128)(2,1)} %param.24, bf16[512,512]{1,0:T(8,128)(2,1)S(1)} %get-tuple-element.6, bf16[512,512]{1,0:T(8,128)(2,1)S(1)} %get-tuple-element.7), kind=kOutput, calls=%fused_computation.7 | convolution fusion | flops 415236096 | bytes 4849664 | tf_op jit(solution)/shard_map/dot_general | solution.py:56
  26.2 10.6 %reshape.119 = f32[16,128,4,256]{3,2,1,0:T(4,128)} reshape(f32[16,128,1024]{2,1,0:T(8,128)} %param.20) | data formatting | bytes 16777216 | tf_op jit(solution)/shard_map/reshape | solution.py:85
  36.8 1.3 fusion.53
  38.6 17.5 %reduce-scatter.2.cloned.1.call-done = f32[16,3072]{1,0:T(8,128)} async-done(((f32[128,3072]{1,0:T(8,128)}), f32[16,3072]{1,0:T(8,128)}) %reduce-scatter.2.cloned.1.call-update) | async-done | bytes 196624 | tf_op jit(solution)/shard_map/reduce_scatter | solution.py:55
  56.1 0.9 convert.9
  57.1 1.4 copy.41
  58.6 0.8 fusion.54
  59.4 6.4 %multiply_add_fusion.1 = f32[16,128,4,256]{3,2,1,0:T(4,128)S(1)} fusion(f32[16,128,4,256]{3,2,1,0:T(4,128)} %reshape.119, f32[16,4,256]{2,1,0:T(4,128)S(1)} %mul.156, f32[16,128,4]{2,1,0:T(8,128)} %copy.41, f32[16,128,4]{2,1,0:T(8,128)S(1)} %copy.40), kind=kLoop, calls=%fused_computation.3 | loop fusion | flops 6291456 | bytes 16908288 | tf_op jit(solution)/shard_map/add | solution.py:92
  65.8 3.4 %fusion = f32[16,4,1,256]{3,2,1,0:T(1,128)S(1)} fusion(f32[16,128,4,256]{3,2,1,0:T(4,128)S(1)} %multiply_add_fusion.1, bf16[16,128,4,1]{1,2,0,3:T(4,128)(2,1)S(1)} %bitcast.89), kind=kOutput, calls=%fused_computation | convolution fusion | flops 25165824 | bytes 8470528 | tf_op jit(solution)/shard_map/skh,skhv->shv/dot_general | solution.py:96
  69.5 8.3 %psum.7 = f32[16,16]{1,0:T(8,128)S(1)} all-reduce(f32[16,16]{1,0:T(8,128)S(1)} %dynamic_update_slice.3), channel_id=1, replica_groups=mesh['ep'=8,'tp'=4] {'tp'}, use_global_device_ids=true, to_apply=%region_3.4 | all-reduce | flops 256 | bytes 2048 | tf_op jit(solution)/shard_map/psum | solution.py:101
  78.0 4.6 %convolution_convert_fusion.1 = bf16[16,4096]{1,0:T(8,128)(2,1)S(1)} fusion(bf16[16,1024]{1,0:T(8,128)(2,1)S(1)} %bitcast.88, bf16[1024,4096]{1,0:T(8,128)(2,1)} %param.30), kind=kOutput, calls=%fused_computation.6 | convolution fusion | flops 134283264 | bytes 8552448 | tf_op jit(solution)/shard_map/dot_general | solution.py:113
  82.7 8.0 %all-gather = bf16[64,4096]{1,0:T(8,128)(2,1)} all-gather(bf16[16,4096]{1,0:T(8,128)(2,1)S(1)} %convolution_convert_fusion.1), channel_id=2, replica_groups=mesh['ep'=8,'tp'=4] {'tp'}, dimensions={0}, use_global_device_ids=true | all-gather | bytes 655360 | tf_op jit(solution)/shard_map/all_gather | solution.py:114
  90.7 1.8 %reduce_sum.70 = bf16[16,4096]{1,0:T(8,128)(2,1)} reduce(bf16[4,16,4096]{2,1,0:T(8,128)(2,1)} %bitcast.86, bf16[]{:T(256)} %constant.69.clone.1), dimensions={0}, to_apply=%region_4.5 | reduce | flops 196608 | bytes 655362 | tf_op jit(solution)/shard_map/reduce_sum | solution.py:114
  92.5 1.1 fusion.33
  93.6 1.2 fusion.2
  94.7 11.6 %all-to-all-start.1 = ((bf16[8,8,4096]{2,1,0:T(8,128)(2,1)}), bf16[8,8,4096]{2,1,0:T(8,128)(2,1)}, u32[]{:S(2)}, u32[]{:S(2)}) async-start(bf16[8,8,4096]{2,1,0:T(8,128)(2,1)} %fusion.2), calls=%async_computation.2 | async-start | bytes 1048576 | tf_op jit(solution)/shard_map/all_to_all | solution.py:142
  106.5 4.5 %mul.153 = f32[16,128,4,256]{3,2,1,0:T(4,128)} broadcast(f32[16,128,4]{2,1,0:T(8,128)S(1)} %copy.40), dimensions={0,1,2} | broadcast | bytes 8421376 | tf_op jit(solution)/shard_map/mul | solution.py:92
  111.0 10.8 %mul.178 = f32[16,128,1024]{2,1,0:T(8,128)} reshape(f32[16,128,4,256]{3,2,1,0:T(4,128)} %mul.153) | data formatting | bytes 16777216 | tf_op jit(solution)/shard_map/mul | solution.py:92
  122.1 4.6 %mul.155 = f32[16,128,4,256]{3,2,1,0:T(4,128)} broadcast(f32[16,128,4]{2,1,0:T(8,128)S(1)} %copy-done.1), dimensions={0,1,2} | broadcast | bytes 8421376 | tf_op jit(solution)/shard_map/mul | solution.py:92
  126.7 10.7 %mul.180 = f32[16,128,1024]{2,1,0:T(8,128)} reshape(f32[16,128,4,256]{3,2,1,0:T(4,128)} %mul.155) | data formatting | bytes 16777216 | tf_op jit(solution)/shard_map/mul | solution.py:92
  137.4 2.5 %fusion.20 = f32[8,1,8,256]{3,2,0,1:T(8,128)S(1)} fusion(bf16[8,8,4096]{2,1,0:T(8,128)(2,1)} %all-to-all-done.1, bf16[1,256,4096]{2,1,0:T(8,128)(2,1)} %param.32), kind=kOutput, calls=%fused_computation.23 | convolution fusion | flops 134217728 | bytes 2686976 | tf_op jit(solution)/shard_map/sxcd,xfd->sxcf/dot_general | solution.py:145
  140.0 2.5 %fusion.29 = bf16[8,1,8,256]{3,2,0,1:T(8,128)(2,1)S(1)} fusion(bf16[8,8,4096]{2,1,0:T(8,128)(2,1)} %all-to-all-done.1, bf16[1,256,4096]{2,1,0:T(8,128)(2,1)} %param.33, f32[8,1,8,256]{3,2,0,1:T(8,128)S(1)} %fusion.20), kind=kOutput, calls=%fused_computation.26 | convolution fusion | flops 134316032 | bytes 2719744 | tf_op jit(solution)/shard_map/sxcd,xfd->sxcf/dot_general | solution.py:148
  142.5 6.8 %all_gather.11 = bf16[8,1,8,1024]{3,2,0,1:T(8,128)(2,1)S(1)} all-gather(bf16[8,1,8,256]{3,2,0,1:T(8,128)(2,1)S(1)} %fusion.29), channel_id=1, replica_groups=mesh['ep'=8,'tp'=4] {'tp'}, dimensions={3}, use_global_device_ids=true | all-gather | bytes 163840 | tf_op jit(solution)/shard_map/all_gather | solution.py:154
  149.3 1.1 fusion.17
  150.5 7.2 %all-to-all-start.2 = ((bf16[8,8,1024]{2,1,0:T(8,128)(2,1)}), bf16[8,8,1024]{2,1,0:T(8,128)(2,1)S(1)}, u32[]{:S(2)}, u32[]{:S(2)}) async-start(bf16[8,8,1024]{2,1,0:T(8,128)(2,1)} %fusion.17), calls=%async_computation.3 | async-start | bytes 262144 | tf_op jit(solution)/shard_map/all_to_all | solution.py:161
  157.6 13.6 %multiply_add_fusion = f32[16,128,1024]{2,1,0:T(8,128)} fusion(f32[16,128,1024]{2,1,0:T(8,128)} %mul.180, f32[16,128,1024]{2,1,0:T(8,128)} %mul.178, f32[16,128,1024]{2,1,0:T(8,128)} %param.20, f32[16,1024]{1,0:T(8,128)S(1)} %get-tuple-element.4), kind=kLoop, calls=%fused_computation.2 | loop fusion | flops 6291456 | bytes 33619968 | tf_op jit(solution)/shard_map/add | solution.py:92
  171.2 0.8 fusion.32
  (53 shorter events, 2.9 us)
Async XLA Ops:
  7.2 142.2 %copy-start = (bf16[1,1024,1024]{2,1,0:T(8,128)(2,1)S(1)}, bf16[1,1024,1024]{2,1,0:T(8,128)(2,1)}, u32[]{:S(2)}) copy-start(bf16[1,1024,1024]{2,1,0:T(8,128)(2,1)} %param.34) | copy-start | bytes 6291460
  10.1 12.1 %all-to-all-start = ((bf16[16,8,512]{2,0,1:T(8,128)(2,1)}), bf16[16,8,512]{2,0,1:T(8,128)(2,1)S(1)}, u32[]{:S(2)}, u32[]{:S(2)}) async-start(bf16[16,8,512]{2,0,1:T(8,128)(2,1)} %bitcast.85), calls=%async_computation | async-start | bytes 262144 | tf_op jit(solution)/shard_map/all_to_all | solution.py:53
  16.4 39.6 %reduce-scatter.2.cloned.1.call-start = ((), (), s32[]{:S(2)}) async-start(), calls=%async_computation.4 | async-start | bytes 1769472 | tf_op jit(solution)/shard_map/reduce_scatter | solution.py:55
  22.2 3.3 %copy-start.5 = (s32[16,2]{0,1:T(2,128)S(1)}, s32[16,2]{0,1:T(2,128)}, u32[]{:S(2)}) copy-start(s32[16,2]{0,1:T(2,128)} %param.35) | copy-start | bytes 388
  26.2 10.6 %copy-start.3 = (bf16[4096,64]{0,1:T(8,128)(2,1)S(1)}, bf16[4096,64]{0,1:T(8,128)(2,1)}, u32[]{:S(2)}) copy-start(bf16[4096,64]{0,1:T(8,128)(2,1)} %param.26) | copy-start | bytes 1572868
  65.8 12.1 %copy-start.6 = (f32[256]{0:T(256)S(1)}, f32[256]{0:T(256)}, u32[]{:S(2)}) copy-start(f32[256]{0:T(256)} %param.29) | copy-start | bytes 3076
  78.0 14.5 %copy-start.2 = (bf16[16,4096]{1,0:T(8,128)(2,1)S(1)}, bf16[16,4096]{1,0:T(8,128)(2,1)}, u32[]{:S(2)}) copy-start(bf16[16,4096]{1,0:T(8,128)(2,1)} %param.19) | copy-start | bytes 393220
  78.0 15.6 %copy-start.4 = (f32[4096]{0:T(1024)S(1)}, f32[4096]{0:T(1024)}, u32[]{:S(2)}) copy-start(f32[4096]{0:T(1024)} %param.31) | copy-start | bytes 49156
  78.0 28.4 %copy-start.7 = (f32[16,2]{0,1:T(2,128)S(1)}, f32[16,2]{0,1:T(2,128)}, u32[]{:S(2)}) copy-start(f32[16,2]{0,1:T(2,128)} %param.36) | copy-start | bytes 388
  78.0 28.4 %copy-start.8 = (f32[16]{0:T(128)S(1)}, f32[16]{0:T(128)}, u32[]{:S(2)}) copy-start(f32[16]{0:T(128)} %param.37) | copy-start | bytes 196
  94.7 42.7 %all-to-all-start.1 = ((bf16[8,8,4096]{2,1,0:T(8,128)(2,1)}), bf16[8,8,4096]{2,1,0:T(8,128)(2,1)}, u32[]{:S(2)}, u32[]{:S(2)}) async-start(bf16[8,8,4096]{2,1,0:T(8,128)(2,1)} %fusion.2), calls=%async_computation.2 | async-start | bytes 1048576 | tf_op jit(solution)/shard_map/all_to_all | solution.py:142
  111.0 11.1 %copy-start.1 = (f32[16,128,4]{2,1,0:T(8,128)S(1)}, f32[16,128,4]{2,1,0:T(8,128)}, u32[]{:S(2)}) copy-start(f32[16,128,4]{2,1,0:T(8,128)} %copy.41) | copy-start | bytes 98308
  150.5 20.8 %all-to-all-start.2 = ((bf16[8,8,1024]{2,1,0:T(8,128)(2,1)}), bf16[8,8,1024]{2,1,0:T(8,128)(2,1)S(1)}, u32[]{:S(2)}, u32[]{:S(2)}) async-start(bf16[8,8,1024]{2,1,0:T(8,128)(2,1)} %fusion.17), calls=%async_computation.3 | async-start | bytes 262144 | tf_op jit(solution)/shard_map/all_to_all | solution.py:161
Sparse Core Ops, SparseCore 0:
  25.7 30.3 reduce-scatter.1
